TPU v7x, 32 devices: a whole 2x2x4 slice. The times are simulated.
32 devices in a mesh: ra: 8 (over z, y), cb: 4 (over x, core).
Axes of the slice: x: 2, y: 2, z: 4, core: 2. Of those that a mesh axis runs over, the one named last changes fastest.
Arguments:
- stream: bfloat16 [64, 1024], P(None, 'ra'), may hold values from -24 to 24, as said below
- gain_first: float32 [1024], P('ra'), may hold values from 0.5 to 1.5
- up_first: float32 [1024, 4096], P('ra', 'cb'), may hold values from -0.1875 to 0.1875
- down_first: float32 [4096, 1024], P('cb', 'ra'), may hold values from -0.09375 to 0.09375
- gain_second: float32 [1024], P('ra'), may hold values from 0.5 to 1.5
- up_second: float32 [1024, 4096], P('ra', 'cb'), may hold values from -0.1875 to 0.1875
- down_second: float32 [4096, 1024], P('cb', 'ra'), may hold values from -0.09375 to 0.09375
Outputs:
- read: bfloat16 [64, 1024], P(None, 'ra')
Inputs may be any that keep to these rules, and one draw needn't show every extreme that they name: stream is of order one, and in each token one aligned block of 128 features is four times larger than the rest.
All inputs are finite; a program needn't handle non-finite values.
Results may differ from a plain program's by a relative error of at most 0.025.
Values may be sent and summed in bfloat16 or wider, within the bound.
A program may use at most 64 MiB of HBM per device.

v0:
```python
import jax
import jax.numpy as jnp
from jax import lax
from jax.sharding import PartitionSpec as P

D = 1024
EPS = 1e-06
RESIDUAL = 0.25


def sublayer(stream, norm_gain, w_up, w_down):
    floated = stream.astype(jnp.float32)
    own_squares = jnp.sum(floated * floated, axis=1, keepdims=True)
    squares = lax.psum(own_squares, "ra")
    factor = lax.rsqrt(squares / D + EPS)
    normed = (floated * factor * norm_gain.astype(jnp.float32)[None, :]).astype(jnp.bfloat16)
    up_bf = w_up.astype(jnp.bfloat16)
    down_bf = w_down.astype(jnp.bfloat16)
    partial_value = jnp.dot(normed, up_bf, preferred_element_type=jnp.float32)
    preact = lax.psum(partial_value, "ra")
    activated = jnp.square(jax.nn.relu(preact)).astype(jnp.bfloat16)
    down_part = jnp.dot(activated, down_bf, preferred_element_type=jnp.float32)
    branch = lax.psum(down_part.astype(jnp.bfloat16), "cb").astype(jnp.float32)
    return (RESIDUAL * floated + branch).astype(jnp.bfloat16)


def local(stream, gain_first, up_first, down_first, gain_second, up_second, down_second):
    middle = sublayer(stream, gain_first, up_first, down_first)
    return sublayer(middle, gain_second, up_second, down_second)


def solution(mesh):
    return jax.shard_map(
        local,
        mesh=mesh,
        in_specs=(
            P(None, "ra"),
            P("ra"),
            P("ra", "cb"),
            P("cb", "ra"),
            P("ra"),
            P("ra", "cb"),
            P("cb", "ra"),
        ),
        out_specs=P(None, "ra"),
        check_vma=False,
    )
```

profile of v0, /device:TPU:0, one launch (start us, length us, event | category | flops | bytes accessed | tf_op | source)
XLA Modules:
  0.0 221.5 jit_solution(7013383935762173612)
XLA Ops:
  6.5 0.0 copy-start.3
  6.5 0.0 all-reduce.3.cloned.1.call-start
  6.5 0.9 fusion.10
  7.4 23.2 %psum.42 = f32[64,1]{0,1:T(1,128)S(1)} all-reduce(f32[64,1]{0,1:T(1,128)S(1)} %bitcast.7), channel_id=1, replica_groups=mesh['ra'=8,'cb'=4] {'ra'}, use_global_device_ids=true, to_apply=%region_1.0 | all-reduce | flops 64 | bytes 512 | tf_op jit(solution)/shard_map/psum | solution.py:14
  30.6 0.0 copy-start.4
  30.6 0.0 copy-done.3
  30.6 0.6 copy-done.4
  31.2 0.0 copy-start.1
  31.2 2.0 fusion.4
  33.3 0.0 copy-start
  33.3 0.0 all-reduce.3.cloned.1.call-update
  33.3 0.0 all-reduce.5.cloned.1.call-start
  33.4 68.4 %all-reduce.3.cloned.1.call-done = f32[64,1024]{1,0:T(8,128)} async-done(((f32[64,1024]{1,0:T(8,128)}), f32[64,1024]{1,0:T(8,128)}) %all-reduce.3.cloned.1.call-update) | async-done | bytes 262160 | tf_op jit(solution)/shard_map/psum | solution.py:20
  101.7 0.0 copy-done.1
  101.7 1.1 convolution_convert_fusion.1
  102.8 10.1 %psum.44 = bf16[64,128]{1,0:T(8,128)(2,1)S(1)} all-reduce(bf16[64,128]{1,0:T(8,128)(2,1)S(1)} %convolution_convert_fusion.1), channel_id=1, replica_groups=mesh['ra'=8,'cb'=4] {'cb'}, use_global_device_ids=true, to_apply=%region_3.4 | all-reduce | flops 8192 | bytes 32768 | tf_op jit(solution)/shard_map/psum | solution.py:23
  113.0 0.1 fusion.15
  113.1 19.6 %psum.45 = f32[64,1]{0,1:T(1,128)S(1)} all-reduce(f32[64,1]{0,1:T(1,128)S(1)} %bitcast.6), channel_id=1, replica_groups=mesh['ra'=8,'cb'=4] {'ra'}, use_global_device_ids=true, to_apply=%region_5.6 | all-reduce | flops 64 | bytes 512 | tf_op jit(solution)/shard_map/psum | solution.py:14
  132.7 0.0 copy-start.5
  132.7 0.0 copy-done
  132.7 0.6 copy-done.5
  133.3 0.0 copy-start.2
  133.3 0.9 fusion.1
  134.3 0.0 all-reduce.5.cloned.1.call-update
  134.3 68.5 %all-reduce.5.cloned.1.call-done = f32[64,1024]{1,0:T(8,128)} async-done(((f32[64,1024]{1,0:T(8,128)}), f32[64,1024]{1,0:T(8,128)}) %all-reduce.5.cloned.1.call-update) | async-done | bytes 262160 | tf_op jit(solution)/shard_map/psum | solution.py:20
  202.8 0.0 copy-done.2
  202.8 1.1 convolution_convert_fusion
  203.9 10.1 %psum.47 = bf16[64,128]{1,0:T(8,128)(2,1)S(1)} all-reduce(bf16[64,128]{1,0:T(8,128)(2,1)S(1)} %convolution_convert_fusion), channel_id=1, replica_groups=mesh['ra'=8,'cb'=4] {'cb'}, use_global_device_ids=true, to_apply=%region_7.8 | all-reduce | flops 8192 | bytes 32768 | tf_op jit(solution)/shard_map/psum | solution.py:23
  214.1 0.6 fusion.14
  (2 shorter events, 0.0 us)
Async XLA Ops:
  6.5 24.1 %copy-start.3 = (bf16[64,128]{1,0:T(8,128)(2,1)S(1)}, bf16[64,128]{1,0:T(8,128)(2,1)}, u32[]{:S(2)}) copy-start(bf16[64,128]{1,0:T(8,128)(2,1)} %param.7) | copy-start | bytes 49156
  6.5 95.2 %all-reduce.3.cloned.1.call-start = ((), (), s32[]{:S(2)}) async-start(), calls=%async_computation | async-start | bytes 524288 | tf_op jit(solution)/shard_map/psum | solution.py:20
  30.6 0.7 copy-start.4
  31.2 70.5 %copy-start.1 = (f32[1024,128]{1,0:T(8,128)S(1)}, f32[1024,128]{1,0:T(8,128)}, u32[]{:S(2)}) copy-start(f32[1024,128]{1,0:T(8,128)} %param.10) | copy-start | bytes 1572868
  33.3 99.4 %copy-start = (f32[128,1024]{1,0:T(8,128)S(1)}, f32[128,1024]{1,0:T(8,128)}, u32[]{:S(2)}) copy-start(f32[128,1024]{1,0:T(8,128)} %param.12) | copy-start | bytes 1572868
  33.3 169.5 %all-reduce.5.cloned.1.call-start = ((), (), s32[]{:S(2)}) async-start(), calls=%async_computation.1 | async-start | bytes 524288 | tf_op jit(solution)/shard_map/psum | solution.py:20
  132.7 0.7 copy-start.5
  133.3 69.5 %copy-start.2 = (f32[1024,128]{1,0:T(8,128)S(1)}, f32[1024,128]{1,0:T(8,128)}, u32[]{:S(2)}) copy-start(f32[1024,128]{1,0:T(8,128)} %param.13) | copy-start | bytes 1572868
Sparse Core Ops, SparseCore 0:
  33.4 68.2 all-reduce.2
  134.4 68.3 all-reduce.4
where the time goes:
time: 222 us
  waiting for transfers between devices  137 us (62%)
  blocking collectives  63 us (28%)
  between operations  13.4 us (6%)
  matrix products  5.2 us (2%)
    psum x2, waiting for transfers between devices, sublayer(): preact = lax.psum(partial_value, 'ra')  137 us
    psum x2, blocking collectives, sublayer(): squares = lax.psum(own_squares, 'ra')  42.8 us
    psum x2, blocking collectives, sublayer(): branch = lax.psum(down_part.astype(jnp.bfloat16), 'cb').astype(jnp.float32)  20.2 us
  transfers between devices with their start and end apart: 2, of which 2 were waited for; matrix products, arithmetic and copies ran while one was open for 0% of the time, Pallas kernels for 0%

commit v1 on v0

--- a/solution.py
+++ b/solution.py
@@ -8,10 +8,19 @@
 RESIDUAL = 0.25
 
 
+def added_up(x, axis):
+    size = lax.axis_size(axis)
+    result, stride = (x, 1)
+    while stride < size:
+        result = result + lax.ppermute(result, axis, [(i, i ^ stride) for i in range(size)])
+        stride = 2 * stride
+    return result
+
+
 def sublayer(stream, norm_gain, w_up, w_down):
     floated = stream.astype(jnp.float32)
     own_squares = jnp.sum(floated * floated, axis=1, keepdims=True)
-    squares = lax.psum(own_squares, "ra")
+    squares = added_up(own_squares, "ra")
     factor = lax.rsqrt(squares / D + EPS)
     normed = (floated * factor * norm_gain.astype(jnp.float32)[None, :]).astype(jnp.bfloat16)
     up_bf = w_up.astype(jnp.bfloat16)

time: 222 us -> 209 us (0.941)
  blocking collectives: 63 us -> 20.2 us
  waiting for transfers between devices: 137 us -> 156 us
  starting transfers between devices: 0.04 us -> 11.6 us
    psum x2 -> x0, blocking collectives: 42.8 us -> none  [sublayer(): squares = lax.psum(own_squares, 'ra')]
    ppermute x0 -> x6, waiting for transfers between devices: none -> 12.9 us  [added_up(): lax.ppermute(result, axis, [(i, i ^ stride) for i in range(size)])]
    ppermute x0 -> x6, starting transfers between devices: none -> 11.5 us  [added_up(): lax.ppermute(result, axis, [(i, i ^ stride) for i in range(size)])]
    psum x2, waiting for transfers between devices: 137 us -> 143 us  [sublayer(): preact = lax.psum(partial_value, 'ra')]
  transfers between devices with their start and end apart: 2 -> 8, of which waited for: 2 -> 8; matrix products, arithmetic and copies ran while one was open for 0% -> 0% of each run, Pallas kernels for 0% -> 0%
where the time goes in v1:
time: 209 us; the launch traced here: 208 us
  waiting for transfers between devices  156 us (75%)
  blocking collectives  20.2 us (10%)
  between operations  13.5 us (6%)
  starting transfers between devices  11.6 us (6%)
  matrix products  5.2 us (2%)
    psum x2, waiting for transfers between devices, sublayer(): preact = lax.psum(partial_value, 'ra')  143 us
    psum x2, blocking collectives, sublayer(): branch = lax.psum(down_part.astype(jnp.bfloat16), 'cb').astype(jnp.float32)  20.2 us
    ppermute x6, waiting for transfers between devices, added_up(): lax.ppermute(result, axis, [(i, i ^ stride) for i in range(size)])  12.9 us
    ppermute x6, starting transfers between devices, added_up(): lax.ppermute(result, axis, [(i, i ^ stride) for i in range(size)])  11.5 us
  transfers between devices with their start and end apart: 8, of which 8 were waited for; matrix products, arithmetic and copies ran while one was open for 0% of the time, Pallas kernels for 0%

profile of v1, /device:TPU:0, one launch (start us, length us, event | category | flops | bytes accessed | tf_op | source)
XLA Modules:
  0.0 208.3 jit_solution(8864792584479702560)
XLA Ops:
  6.5 0.0 copy-start.3
  6.5 0.0 all-reduce.3.cloned.1.call-start
  6.5 0.9 fusion.10
  7.4 3.1 %collective-permute-start = (f32[64,1]{0,1:T(1,128)S(1)}, f32[64,1]{0,1:T(1,128)S(1)}, u32[]{:S(2)}, u32[]{:S(2)}) collective-permute-start(f32[64,1]{0,1:T(1,128)S(1)} %bitcast.9), channel_id=1, source_target_pairs={{0,4},{4,0},{8,12},{12,8},{16,20},{20,16},{24,28},{28,24},{1,5},{5... | collective-permute-start | bytes 776 | tf_op jit(solution)/shard_map/ppermute | solution.py:15
  10.5 1.5 collective-permute-done
  12.0 2.1 collective-permute-start.1
  14.1 1.5 collective-permute-done.1
  15.7 0.0 copy-start.4
  15.7 3.0 %collective-permute-start.2 = (f32[64,1]{0,1:T(1,128)S(1)}, f32[64,1]{0,1:T(1,128)S(1)}, u32[]{:S(2)}, u32[]{:S(2)}) collective-permute-start(f32[64,1]{0,1:T(1,128)S(1)} %add.39), channel_id=1, source_target_pairs={{0,16},{4,20},{8,24},{12,28},{16,0},{20,4},{24,8},{28,12},{1,17},{... | collective-permute-start | bytes 776 | tf_op jit(solution)/shard_map/ppermute | solution.py:15
  18.7 1.5 collective-permute-done.2
  20.3 0.0 copy-done.3
  20.3 0.0 copy-done.4
  20.3 0.0 copy-start.1
  20.3 2.0 fusion.4
  22.3 0.0 copy-start
  22.3 0.0 all-reduce.3.cloned.1.call-update
  22.3 0.0 all-reduce.5.cloned.1.call-start
  22.4 72.7 %all-reduce.3.cloned.1.call-done = f32[64,1024]{1,0:T(8,128)} async-done(((f32[64,1024]{1,0:T(8,128)}), f32[64,1024]{1,0:T(8,128)}) %all-reduce.3.cloned.1.call-update) | async-done | bytes 262160 | tf_op jit(solution)/shard_map/psum | solution.py:29
  95.1 0.0 copy-done.1
  95.1 1.1 convolution_convert_fusion.1
  96.2 10.1 %psum.29 = bf16[64,128]{1,0:T(8,128)(2,1)S(1)} all-reduce(bf16[64,128]{1,0:T(8,128)(2,1)S(1)} %convolution_convert_fusion.1), channel_id=1, replica_groups=mesh['ra'=8,'cb'=4] {'cb'}, use_global_device_ids=true, to_apply=%region_2.3 | all-reduce | flops 8192 | bytes 32768 | tf_op jit(solution)/shard_map/psum | solution.py:32
  106.3 0.1 fusion.15
  106.4 0.7 collective-permute-start.3
  107.2 2.9 %collective-permute-done.3 = f32[64,1]{0,1:T(1,128)S(1)} collective-permute-done((f32[64,1]{0,1:T(1,128)S(1)}, f32[64,1]{0,1:T(1,128)S(1)}, u32[]{:S(2)}, u32[]{:S(2)}) %collective-permute-start.3) | collective-permute-done | bytes 288 | tf_op jit(solution)/shard_map/ppermute | solution.py:15
  110.1 1.0 collective-permute-start.4
  111.1 2.6 %collective-permute-done.4 = f32[64,1]{0,1:T(1,128)S(1)} collective-permute-done((f32[64,1]{0,1:T(1,128)S(1)}, f32[64,1]{0,1:T(1,128)S(1)}, u32[]{:S(2)}, u32[]{:S(2)}) %collective-permute-start.4) | collective-permute-done | bytes 288 | tf_op jit(solution)/shard_map/ppermute | solution.py:15
  113.6 0.0 copy-start.5
  113.6 1.7 collective-permute-start.5
  115.3 2.8 %collective-permute-done.5 = f32[64,1]{0,1:T(1,128)S(1)} collective-permute-done((f32[64,1]{0,1:T(1,128)S(1)}, f32[64,1]{0,1:T(1,128)S(1)}, u32[]{:S(2)}, u32[]{:S(2)}) %collective-permute-start.5) | collective-permute-done | bytes 288 | tf_op jit(solution)/shard_map/ppermute | solution.py:15
  118.1 0.0 copy-done
  118.1 0.0 copy-done.5
  118.1 0.0 copy-start.2
  118.1 0.9 fusion.1
  119.1 0.0 all-reduce.5.cloned.1.call-update
  119.1 70.5 %all-reduce.5.cloned.1.call-done = f32[64,1024]{1,0:T(8,128)} async-done(((f32[64,1024]{1,0:T(8,128)}), f32[64,1024]{1,0:T(8,128)}) %all-reduce.5.cloned.1.call-update) | async-done | bytes 262160 | tf_op jit(solution)/shard_map/psum | solution.py:29
  189.6 0.0 copy-done.2
  189.6 1.1 convolution_convert_fusion
  190.7 10.1 %psum.31 = bf16[64,128]{1,0:T(8,128)(2,1)S(1)} all-reduce(bf16[64,128]{1,0:T(8,128)(2,1)S(1)} %convolution_convert_fusion), channel_id=1, replica_groups=mesh['ra'=8,'cb'=4] {'cb'}, use_global_device_ids=true, to_apply=%region_5.6 | all-reduce | flops 8192 | bytes 32768 | tf_op jit(solution)/shard_map/psum | solution.py:32
  200.8 0.6 fusion.14
  (6 shorter events, 0.0 us)
Async XLA Ops:
  6.5 13.7 %copy-start.3 = (bf16[64,128]{1,0:T(8,128)(2,1)S(1)}, bf16[64,128]{1,0:T(8,128)(2,1)}, u32[]{:S(2)}) copy-start(bf16[64,128]{1,0:T(8,128)(2,1)} %param.7) | copy-start | bytes 49156
  6.5 88.5 %all-reduce.3.cloned.1.call-start = ((), (), s32[]{:S(2)}) async-start(), calls=%async_computation | async-start | bytes 524288 | tf_op jit(solution)/shard_map/psum | solution.py:29
  7.4 4.6 %collective-permute-start = (f32[64,1]{0,1:T(1,128)S(1)}, f32[64,1]{0,1:T(1,128)S(1)}, u32[]{:S(2)}, u32[]{:S(2)}) collective-permute-start(f32[64,1]{0,1:T(1,128)S(1)} %bitcast.9), channel_id=1, source_target_pairs={{0,4},{4,0},{8,12},{12,8},{16,20},{20,16},{24,28},{28,24},{1,5},{5... | collective-permute-start | bytes 776 | tf_op jit(solution)/shard_map/ppermute | solution.py:15
  12.0 3.6 %collective-permute-start.1 = (f32[64,1]{0,1:T(1,128)S(1)}, f32[64,1]{0,1:T(1,128)S(1)}, u32[]{:S(2)}, u32[]{:S(2)}) collective-permute-start(f32[64,1]{0,1:T(1,128)S(1)} %bitcast_add_fusion.1), channel_id=1, source_target_pairs={{0,8},{4,12},{8,0},{12,4},{16,24},{20,28},{24,16},{28,20},{1,9},{5... | collective-permute-start | bytes 776 | tf_op jit(solution)/shard_map/ppermute | solution.py:15
  15.7 4.6 %copy-start.4 = (f32[128]{0:T(128)S(1)}, f32[128]{0:T(128)}, u32[]{:S(2)}) copy-start(f32[128]{0:T(128)} %param.8) | copy-start | bytes 1540
  15.7 4.6 %collective-permute-start.2 = (f32[64,1]{0,1:T(1,128)S(1)}, f32[64,1]{0,1:T(1,128)S(1)}, u32[]{:S(2)}, u32[]{:S(2)}) collective-permute-start(f32[64,1]{0,1:T(1,128)S(1)} %add.39), channel_id=1, source_target_pairs={{0,16},{4,20},{8,24},{12,28},{16,0},{20,4},{24,8},{28,12},{1,17},{... | collective-permute-start | bytes 776 | tf_op jit(solution)/shard_map/ppermute | solution.py:15
  20.3 74.8 %copy-start.1 = (f32[1024,128]{1,0:T(8,128)S(1)}, f32[1024,128]{1,0:T(8,128)}, u32[]{:S(2)}) copy-start(f32[1024,128]{1,0:T(8,128)} %param.10) | copy-start | bytes 1572868
  22.3 95.8 %copy-start = (f32[128,1024]{1,0:T(8,128)S(1)}, f32[128,1024]{1,0:T(8,128)}, u32[]{:S(2)}) copy-start(f32[128,1024]{1,0:T(8,128)} %param.12) | copy-start | bytes 1572868
  22.3 167.2 %all-reduce.5.cloned.1.call-start = ((), (), s32[]{:S(2)}) async-start(), calls=%async_computation.1 | async-start | bytes 524288 | tf_op jit(solution)/shard_map/psum | solution.py:29
  106.4 3.6 %collective-permute-start.3 = (f32[64,1]{0,1:T(1,128)S(1)}, f32[64,1]{0,1:T(1,128)S(1)}, u32[]{:S(2)}, u32[]{:S(2)}) collective-permute-start(f32[64,1]{0,1:T(1,128)S(1)} %bitcast.8), channel_id=1, source_target_pairs={{0,4},{4,0},{8,12},{12,8},{16,20},{20,16},{24,28},{28,24},{1,5},{5... | collective-permute-start | bytes 776 | tf_op jit(solution)/shard_map/ppermute | solution.py:15
  110.1 3.6 %collective-permute-start.4 = (f32[64,1]{0,1:T(1,128)S(1)}, f32[64,1]{0,1:T(1,128)S(1)}, u32[]{:S(2)}, u32[]{:S(2)}) collective-permute-start(f32[64,1]{0,1:T(1,128)S(1)} %bitcast_add_fusion), channel_id=1, source_target_pairs={{0,8},{4,12},{8,0},{12,4},{16,24},{20,28},{24,16},{28,20},{1,9},{5... | collective-permute-start | bytes 776 | tf_op jit(solution)/shard_map/ppermute | solution.py:15
  113.6 4.5 %copy-start.5 = (f32[128]{0:T(128)S(1)}, f32[128]{0:T(128)}, u32[]{:S(2)}) copy-start(f32[128]{0:T(128)} %param.11) | copy-start | bytes 1540
  113.6 4.5 %collective-permute-start.5 = (f32[64,1]{0,1:T(1,128)S(1)}, f32[64,1]{0,1:T(1,128)S(1)}, u32[]{:S(2)}, u32[]{:S(2)}) collective-permute-start(f32[64,1]{0,1:T(1,128)S(1)} %add.44), channel_id=1, source_target_pairs={{0,16},{4,20},{8,24},{12,28},{16,0},{20,4},{24,8},{28,12},{1,17},{... | collective-permute-start | bytes 776 | tf_op jit(solution)/shard_map/ppermute | solution.py:15
  118.1 71.5 %copy-start.2 = (f32[1024,128]{1,0:T(8,128)S(1)}, f32[1024,128]{1,0:T(8,128)}, u32[]{:S(2)}) copy-start(f32[1024,128]{1,0:T(8,128)} %param.13) | copy-start | bytes 1572868
Sparse Core Ops, SparseCore 0:
  22.5 72.5 all-reduce.2
  119.2 70.3 all-reduce.4
